TPU v7x, 32 devices: a whole 2x2x4 slice. The times are simulated.
32 devices in a mesh: ep: 16 (over z, y, x), tp: 2 (over core).
Axes of the slice: x: 2, y: 2, z: 4, core: 2. Of those that a mesh axis runs over, the one named last changes fastest.
Arguments:
- tokens: bfloat16 [256, 2048], P('ep'), may hold values from -6 to 6
- mix_gain: float32 [2048], replicated, may hold values from 0.1 to 1.9
- query_weight: bfloat16 [2048, 1024], P('ep', 'tp'), may hold values from -0.125 to 0.125
- forget_weight: bfloat16 [2048, 1024], P('ep', 'tp'), may hold values from -0.125 to 0.125
- input_weight: bfloat16 [2048, 1024], P('ep', 'tp'), may hold values from -0.125 to 0.125
- lower_bound: float32 [1024], P('tp'), may hold values from 0 to 0.9
- head_gain: float32 [1024], P('tp'), may hold values from 0.1 to 1.9
- out_weight: bfloat16 [1024, 2048], P('tp', 'ep'), may hold values from -0.1875 to 0.1875
- state: float32 [256, 8, 128, 128], P('ep', 'tp'), may hold values from -4 to 4
- ffn_gain: float32 [2048], replicated, may hold values from 0.1 to 1.9
- route_ids: int32 [256, 2], P('ep'), may hold values from 0 to 7, all different within a row; in each aligned block of 16 rows (0 to 15, 16 to 31, ...) at most 6 rows name the same one
- route_weights: float32 [256, 2], P('ep'), may hold values from 0.25 to 1
- expert_gate: bfloat16 [16, 2048, 2048], P('ep', None, 'tp'), may hold values from -0.125 to 0.125
- expert_up: bfloat16 [16, 2048, 2048], P('ep', None, 'tp'), may hold values from -0.125 to 0.125
- expert_down: bfloat16 [16, 2048, 2048], P('ep', 'tp'), may hold values from -0.09375 to 0.09375
Outputs:
- mixed_out: bfloat16 [256, 2048], P('ep', 'tp')
- new_state: float32 [256, 8, 128, 128], P('ep', 'tp')
Inputs may be any that keep to these rules, and one draw needn't show every extreme that they name: `route_ids`: each row names 2 different experts; among the rows of one device no expert is named by more than 6 rows, a bound that some block reaches of them.
All inputs are finite; a program needn't handle non-finite values.
Results may differ from a plain program's by a relative error of at most 0.015.
Values may be sent and summed in bfloat16 or wider, within the bound.
A program may use at most 64 MiB of HBM per device.

v0:
```python
import jax
import jax.numpy as jnp
from jax import lax
from jax.sharding import PartitionSpec as P

EXPERTS = 8
TOP = 2
epsilon = 1e-06


def rms_scale(values_in, gain_vec):
    return (
        values_in
        * lax.rsqrt(jnp.mean(values_in * values_in, axis=-1, keepdims=True) + epsilon)
        * gain_vec
    )


def slot_ranks(block_ids, expert_count):
    onehot = (block_ids[..., None] == jnp.arange(expert_count, dtype=jnp.int32)).astype(jnp.int32)
    before = jnp.cumsum(onehot, axis=1) - onehot
    return jnp.sum(before * onehot, axis=-1)


def shards(
    tokens,
    mix_gain,
    query_weight,
    forget_weight,
    input_weight,
    lower_bound,
    head_gain,
    out_weight,
    state,
    ffn_gain,
    route_ids,
    route_weights,
    expert_gate,
    expert_up,
    expert_down,
):
    seq_dev = tokens.shape[0]
    model_width = tokens.shape[1]
    ep_count = lax.axis_size("ep")
    residual = tokens.astype(jnp.float32)
    normed = rms_scale(residual, mix_gain).astype(jnp.bfloat16)
    head_count = state.shape[1]
    head_size = state.shape[2]
    proj_width = query_weight.shape[1]
    pieces = (
        lax.all_gather(query_weight, "ep", axis=0, tiled=True),
        lax.all_gather(forget_weight, "ep", axis=0, tiled=True),
        lax.all_gather(input_weight, "ep", axis=0, tiled=True),
    )
    queries, forget_pre, fresh_values = tuple(
        (jnp.dot(normed, weight_rows, preferred_element_type=jnp.float32) for weight_rows in pieces)
    )
    forget = (lower_bound + (1.0 - lower_bound) * jax.nn.sigmoid(forget_pre)).reshape(
        seq_dev, head_count, head_size
    )
    queries = queries.reshape(seq_dev, head_count, head_size)
    fresh_values = fresh_values.reshape(seq_dev, head_count, head_size)
    new_state = forget[..., None] * state + (1.0 - forget)[..., None] * fresh_values[:, :, None, :]
    readout = jnp.einsum("shk,shkv->shv", queries, new_state, precision=lax.Precision.HIGHEST)
    readout = rms_scale(readout, head_gain.reshape(head_count, head_size))
    heads_out = readout.reshape(seq_dev, proj_width).astype(jnp.bfloat16)
    partial_mix = jnp.dot(
        heads_out,
        lax.all_gather(out_weight, "ep", axis=1, tiled=True),
        preferred_element_type=jnp.float32,
    )
    mixer_sum = lax.psum(partial_mix.astype(jnp.bfloat16), "tp").astype(jnp.float32)
    after_mixer = (residual + mixer_sum).astype(jnp.bfloat16)
    ffn_in = rms_scale(after_mixer.astype(jnp.float32), ffn_gain).astype(jnp.bfloat16)
    capacity = 3 * seq_dev // 8
    expert_span = ep_count // EXPERTS
    half_width = model_width // lax.axis_size("tp")
    own_columns = lax.dynamic_slice_in_dim(
        after_mixer, lax.axis_index("tp") * half_width, half_width, 1
    ).astype(jnp.float32)
    gate_slice = expert_gate[0]
    up_slice = expert_up[0]
    down_slice = expert_down[0]
    slot_iota = jnp.arange(capacity, dtype=jnp.int32)
    own_rank = slot_ranks(route_ids.reshape(1, seq_dev * TOP), EXPERTS).reshape(seq_dev, TOP)
    expert_iota = jnp.arange(EXPERTS, dtype=jnp.int32)
    chosen = (route_ids[:, :, None, None] == expert_iota[None, None, :, None]) & (
        own_rank[:, :, None, None] == slot_iota[None, None, None, :]
    )
    dispatch = jnp.any(chosen, axis=1).astype(jnp.bfloat16)
    combine = jnp.sum(chosen.astype(jnp.float32) * route_weights[:, :, None, None], axis=1)
    outgoing = jnp.einsum(
        "tec,td->ecd", dispatch, ffn_in, preferred_element_type=jnp.float32
    ).astype(jnp.bfloat16)
    outgoing = jnp.broadcast_to(
        outgoing[:, None], (EXPERTS, expert_span, capacity, model_width)
    ).reshape(ep_count, capacity, model_width)
    slot_rows = lax.all_to_all(outgoing, "ep", split_axis=0, concat_axis=0, tiled=True)
    gate_pre = jnp.einsum(
        "...d,df->...f", slot_rows, gate_slice, preferred_element_type=jnp.float32
    )
    up_pre = jnp.einsum("...d,df->...f", slot_rows, up_slice, preferred_element_type=jnp.float32)
    hidden = (jax.nn.silu(gate_pre) * up_pre).astype(jnp.bfloat16)
    partial_out = jnp.einsum(
        "...f,fd->...d", hidden, down_slice, preferred_element_type=jnp.float32
    )
    reduced = lax.psum_scatter(
        partial_out.astype(jnp.bfloat16), "tp", scatter_dimension=2, tiled=True
    ).astype(jnp.float32)
    returned = lax.all_to_all(
        reduced.astype(jnp.bfloat16), "ep", split_axis=0, concat_axis=0, tiled=True
    ).astype(reduced.dtype)
    expert_out = jnp.sum(returned.reshape(EXPERTS, expert_span, capacity, half_width), axis=1)
    expert_mix = jnp.einsum("tec,ecd->td", combine, expert_out, precision=lax.Precision.HIGHEST)
    mixed_out = (own_columns + expert_mix).astype(jnp.bfloat16)
    return (mixed_out, new_state)


def solution(mesh):
    return jax.shard_map(
        shards,
        mesh=mesh,
        in_specs=(
            P("ep", None),
            P(),
            P("ep", "tp"),
            P("ep", "tp"),
            P("ep", "tp"),
            P("tp"),
            P("tp"),
            P("tp", "ep"),
            P("ep", "tp", None, None),
            P(),
            P("ep", None),
            P("ep", None),
            P("ep", None, "tp"),
            P("ep", None, "tp"),
            P("ep", "tp", None),
        ),
        out_specs=(P("ep", "tp"), P("ep", "tp", None, None)),
        check_vma=False,
    )
```

profile of v0, /device:TPU:0, one launch (start us, length us, event | category | flops | bytes accessed | tf_op | source)
XLA Modules:
  0.0 346.5 jit_solution(2052995556414389581)
XLA Ops:
  8.0 0.7 all-gather.9.cloned.1.call-update
  10.0 0.8 copy.47
  11.4 1.0 fusion.37
  13.7 60.2 %all-gather.7.cloned.1.call-done = bf16[2048,512]{1,0:T(8,128)(2,1)} async-done(((bf16[128,512]{1,0:T(8,128)(2,1)}), bf16[2048,512]{1,0:T(8,128)(2,1)}) %all-gather.7.cloned.1.call-update) | async-done | bytes 2097168 | tf_op jit(solution)/shard_map/all_gather | solution.py:52
  73.9 2.1 fusion.21
  76.0 59.9 %all-gather.9.cloned.1.call-done = bf16[2048,512]{1,0:T(8,128)(2,1)} async-done(((bf16[128,512]{1,0:T(8,128)(2,1)}), bf16[2048,512]{1,0:T(8,128)(2,1)}) %all-gather.9.cloned.1.call-update) | async-done | bytes 2097168 | tf_op jit(solution)/shard_map/all_gather | solution.py:53
  135.9 2.1 fusion.50
  138.0 59.9 %all-gather.5.cloned.1.call-done = bf16[2048,512]{1,0:T(8,128)(2,1)} async-done(((bf16[128,512]{1,0:T(8,128)(2,1)}), bf16[2048,512]{1,0:T(8,128)(2,1)}) %all-gather.5.cloned.1.call-update) | async-done | bytes 2097168 | tf_op jit(solution)/shard_map/all_gather | solution.py:51
  197.9 2.0 fusion.53
  199.9 4.4 %multiply_add_fusion = f32[16,4,128,128]{3,2,1,0:T(8,128)S(1)} fusion(f32[16,4,128,128]{3,2,1,0:T(8,128)} %param.23, f32[16,4,128]{2,1,0:T(4,128)S(1)} %mul.124, f32[16,4,128]{2,1,0:T(4,128)S(1)} %broadcast_subtract_fusion, f32[16,4,128]{2,1,0:T(4,128)S(1)} %mul.120), kind=kLoop, calls=%fused_computation.6 | loop fusion | flops 3145728 | bytes 8486912 | tf_op jit(solution)/shard_map/add | solution.py:63
  204.4 2.0 copy-done
  206.3 3.7 %fusion.56 = f32[16,4,1,128]{3,2,1,0:T(1,128)S(1)} fusion(f32[16,4,128,1]{2,3,1,0:T(1,128)S(1)} %bitcast.52, f32[16,4,128,128]{3,2,1,0:T(8,128)S(1)} %multiply_add_fusion), kind=kOutput, calls=%fused_computation.66 | convolution fusion | flops 12582912 | bytes 4259840 | tf_op jit(solution)/shard_map/shk,shkv->shv/dot_general | solution.py:64
  210.2 52.0 %all-gather.11.cloned.1.call-done = bf16[512,2048]{1,0:T(8,128)(2,1)} async-done(((bf16[512,128]{1,0:T(8,128)(2,1)}), bf16[512,2048]{1,0:T(8,128)(2,1)}) %all-gather.11.cloned.1.call-update) | async-done | bytes 2097168 | tf_op jit(solution)/shard_map/all_gather | solution.py:69
  262.2 2.6 convolution_convert_fusion.1
  264.9 16.0 %all-reduce.2.cloned.1.call-done = bf16[16,2048]{1,0:T(8,128)(2,1)} async-done(((bf16[16,2048]{1,0:T(8,128)(2,1)}), bf16[16,2048]{1,0:T(8,128)(2,1)}) %all-reduce.2.cloned.1.call-update) | async-done | bytes 65552 | tf_op jit(solution)/shard_map/psum | solution.py:72
  280.9 1.0 fusion.34
  282.3 22.1 %all_to_all.10 = bf16[16,6,2048]{2,1,0:T(8,128)(2,1)S(1)} all-to-all(bf16[16,6,2048]{2,1,0:T(8,128)(2,1)S(1)} %bitcast.49), channel_id=1, replica_groups=mesh['ep'=16,'tp'=2] {'ep'}, dimensions={0} | all-to-all | bytes 786432 | tf_op jit(solution)/shard_map/all_to_all | solution.py:98
  304.4 3.1 fusion.4
  307.5 5.9 %fusion.6 = bf16[16,6,2048]{2,0,1:T(8,128)(2,1)} fusion(bf16[1,1024,2048]{2,1,0:T(8,128)(2,1)} %param.29, bf16[1,2048,1024]{2,1,0:T(8,128)(2,1)} %param.28, f32[16,6,1024]{2,0,1:T(8,128)S(1)} %fusion.4, bf16[16,6,2048]{2,1,0:T(8,128)(2,1)S(1)} %all_to_all.10), kind=kOutput, calls=%fused_computation.7 | convolution fusion | flops 806092800 | bytes 9568256 | tf_op jit(solution)/shard_map/...f,fd->...d/dot_general | solution.py:104
  313.4 6.3 %reduce-scatter.2.cloned.1.call-done = bf16[16,6,1024]{2,0,1:T(8,128)(2,1)} async-done(((bf16[16,6,2048]{2,0,1:T(8,128)(2,1)}), bf16[16,6,1024]{2,0,1:T(8,128)(2,1)}) %reduce-scatter.2.cloned.1.call-update) | async-done | bytes 196624 | tf_op jit(solution)/shard_map/reduce_scatter | solution.py:107
  319.8 1.7 copy.52
  321.5 6.7 %all-to-all-start.1 = ((bf16[16,6,1024]{2,1,0:T(8,128)(2,1)}), bf16[16,6,1024]{2,1,0:T(8,128)(2,1)S(1)}, u32[]{:S(2)}, u32[]{:S(2)}) async-start(bf16[16,6,1024]{2,1,0:T(8,128)(2,1)} %copy.52), calls=%async_computation.2 | async-start | bytes 524288 | tf_op jit(solution)/shard_map/all_to_all | solution.py:110
  328.3 10.4 %all-to-all-done.1 = bf16[16,6,1024]{2,1,0:T(8,128)(2,1)S(1)} async-done(((bf16[16,6,1024]{2,1,0:T(8,128)(2,1)}), bf16[16,6,1024]{2,1,0:T(8,128)(2,1)S(1)}, u32[]{:S(2)}, u32[]{:S(2)}) %all-to-all-start.1) | async-done | bytes 196640 | tf_op jit(solution)/shard_map/all_to_all | solution.py:110
  338.7 0.9 fusion.16
  (46 shorter events, 4.9 us)
Async XLA Ops:
  7.2 190.7 %copy-start.1 = (bf16[16,2048]{1,0:T(8,128)(2,1)S(1)}, bf16[16,2048]{1,0:T(8,128)(2,1)}, u32[]{:S(2)}) copy-start(bf16[16,2048]{1,0:T(8,128)(2,1)} %param.15) | copy-start | bytes 196612
  7.2 190.7 %copy-start.2 = (f32[2048]{0:T(1024)S(1)}, f32[2048]{0:T(1024)}, u32[]{:S(2)}) copy-start(f32[2048]{0:T(1024)} %param.16) | copy-start | bytes 24580
  7.2 66.7 %all-gather.7.cloned.1.call-start = ((), (), s32[]{:S(2)}) async-start(), calls=%async_computation.4 | async-start | bytes 2228224 | tf_op jit(solution)/shard_map/all_gather | solution.py:52
  7.9 128.0 %all-gather.9.cloned.1.call-start = ((), (), s32[]{:S(2)}) async-start(), calls=%async_computation.5 | async-start | bytes 2228224 | tf_op jit(solution)/shard_map/all_gather | solution.py:53
  8.7 189.2 %all-gather.5.cloned.1.call-start = ((), (), s32[]{:S(2)}) async-start(), calls=%async_computation.3 | async-start | bytes 2228224 | tf_op jit(solution)/shard_map/all_gather | solution.py:51
  9.4 252.8 %all-gather.11.cloned.1.call-start = ((), (), s32[]{:S(2)}) async-start(), calls=%async_computation.6 | async-start | bytes 2228224 | tf_op jit(solution)/shard_map/all_gather | solution.py:69
  10.0 270.9 %all-reduce.2.cloned.1.call-start = ((), (), s32[]{:S(2)}) async-start(), calls=%async_computation.7 | async-start | bytes 131072 | tf_op jit(solution)/shard_map/psum | solution.py:72
  204.3 2.0 copy-start
  204.3 5.8 %copy-start.4 = (f32[512]{0:T(512)S(1)}, f32[512]{0:T(512)}, u32[]{:S(2)}) copy-start(f32[512]{0:T(512)} %param.21) | copy-start | bytes 6148
  204.4 77.5 %copy-start.3 = (f32[2048]{0:T(1024)S(1)}, f32[2048]{0:T(1024)}, u32[]{:S(2)}) copy-start(f32[2048]{0:T(1024)} %param.24) | copy-start | bytes 24580
  264.8 55.0 %reduce-scatter.2.cloned.1.call-start = ((), (), s32[]{:S(2)}) async-start(), calls=%async_computation.8 | async-start | bytes 589824 | tf_op jit(solution)/shard_map/reduce_scatter | solution.py:107
  307.5 20.7 %copy-start.5 = (f32[16,2]{0,1:T(2,128)S(1)}, f32[16,2]{0,1:T(2,128)}, u32[]{:S(2)}) copy-start(f32[16,2]{0,1:T(2,128)} %param.26) | copy-start | bytes 388
  321.5 17.1 %all-to-all-start.1 = ((bf16[16,6,1024]{2,1,0:T(8,128)(2,1)}), bf16[16,6,1024]{2,1,0:T(8,128)(2,1)S(1)}, u32[]{:S(2)}, u32[]{:S(2)}) async-start(bf16[16,6,1024]{2,1,0:T(8,128)(2,1)} %copy.52), calls=%async_computation.2 | async-start | bytes 524288 | tf_op jit(solution)/shard_map/all_to_all | solution.py:110
Sparse Core Ops, SparseCore 0:
  10.8 63.0 all-gather.6
  76.7 59.1 all-gather.8
  138.7 59.1 all-gather.4
  200.4 61.7 all-gather.10
  264.9 15.8 all-reduce.1
  313.6 6.1 reduce-scatter.1
where the time goes:
time: 347 us; the launch traced here: 346 us
  waiting for transfers between devices  267 us (77%)
  matrix products  22.6 us (7%)
  blocking collectives  22.1 us (6%)
  between operations  14.3 us (4%)
  other arithmetic  8.35 us (2%)
  starting transfers between devices  6.96 us (2%)
  local copies, waits for them, and re-layouts  4.97 us (1%)
    all_gather x1, waiting for transfers between devices, shards(): lax.all_gather(forget_weight, 'ep', axis=0, tiled=True)  60.2 us
    all_gather x1, waiting for transfers between devices, shards(): lax.all_gather(query_weight, 'ep', axis=0, tiled=True)  59.9 us
    all_gather x1, waiting for transfers between devices, shards(): lax.all_gather(input_weight, 'ep', axis=0, tiled=True)  59.9 us
    all_gather x1, waiting for transfers between devices, shards(): lax.all_gather(out_weight, 'ep', axis=1, tiled=True)  52 us
    all_to_all x1, blocking collectives, shards(): lax.all_to_all(outgoing, 'ep', split_axis=0, concat_axis=0, tiled=True)  22.1 us
    psum x1, waiting for transfers between devices, shards(): lax.psum(partial_mix.astype(jnp.bfloat16), 'tp').astype(jnp.float32)  16 us
    all_to_all x1, waiting for transfers between devices, shards(): lax.all_to_all(reduced.astype(jnp.bfloat16), 'ep', split_axis=0, concat_a...  10.4 us
  transfers between devices with their start and end apart: 7, of which 7 were waited for; matrix products, arithmetic and copies ran while one was open for 5% of the time, Pallas kernels for 0%

commit v1 on v0

--- a/solution.py
+++ b/solution.py
@@ -66,7 +66,7 @@
     heads_out = readout.reshape(seq_dev, proj_width).astype(jnp.bfloat16)
     partial_mix = jnp.dot(
         heads_out,
-        lax.all_gather(out_weight, "ep", axis=1, tiled=True),
+        jnp.concatenate(lax.all_gather(out_weight, "ep"), axis=1),
         preferred_element_type=jnp.float32,
     )
     mixer_sum = lax.psum(partial_mix.astype(jnp.bfloat16), "tp").astype(jnp.float32)

time: 347 us -> 356 us (1.026)
  waiting for transfers between devices: 267 us -> 275 us
    all_gather x1, waiting for transfers between devices: 52 us -> 60.2 us  [shards(): lax.all_gather(out_weight, 'ep')]
  transfers between devices with their start and end apart: 7 -> 7, of which waited for: 7 -> 7; matrix products, arithmetic and copies ran while one was open for 5% -> 3% of each run, Pallas kernels for 0% -> 0%
where the time goes in v1:
time: 356 us
  waiting for transfers between devices  275 us (77%)
  blocking collectives  22.1 us (6%)
  matrix products  21.1 us (6%)
  between operations  14.3 us (4%)
  other arithmetic  8.34 us (2%)
  local copies, waits for them, and re-layouts  7.84 us (2%)
  starting transfers between devices  6.95 us (2%)
    all_gather x1, waiting for transfers between devices, shards(): lax.all_gather(out_weight, 'ep')  60.2 us
    all_gather x1, waiting for transfers between devices, shards(): lax.all_gather(input_weight, 'ep', axis=0, tiled=True)  59.9 us
    all_gather x1, waiting for transfers between devices, shards(): lax.all_gather(forget_weight, 'ep', axis=0, tiled=True)  59.8 us
    all_gather x1, waiting for transfers between devices, shards(): lax.all_gather(query_weight, 'ep', axis=0, tiled=True)  59.1 us
    all_to_all x1, blocking collectives, shards(): lax.all_to_all(outgoing, 'ep', split_axis=0, concat_axis=0, tiled=True)  22.1 us
    psum x1, waiting for transfers between devices, shards(): lax.psum(partial_mix.astype(jnp.bfloat16), 'tp').astype(jnp.float32)  16.6 us
    all_to_all x1, waiting for transfers between devices, shards(): lax.all_to_all(reduced.astype(jnp.bfloat16), 'ep', split_axis=0, concat_a...  10.3 us
  transfers between devices with their start and end apart: 7, of which 7 were waited for; matrix products, arithmetic and copies ran while one was open for 3% of the time, Pallas kernels for 0%

profile of v1, /device:TPU:0, one launch (start us, length us, event | category | flops | bytes accessed | tf_op | source)
XLA Modules:
  0.0 355.6 jit_solution(10672729184195997613)
XLA Ops:
  10.0 0.8 copy.55
  11.4 1.0 fusion.37
  13.7 60.2 %all-gather.12.cloned.1.call-done = bf16[8192,128]{1,0:T(8,128)(2,1)} async-done(((bf16[512,128]{1,0:T(8,128)(2,1)}), bf16[8192,128]{1,0:T(8,128)(2,1)}) %all-gather.12.cloned.1.call-update) | async-done | bytes 2097168 | tf_op jit(solution)/shard_map/all_gather | solution.py:69
  73.9 2.9 copy.54
  76.8 59.1 %all-gather.6.cloned.1.call-done = bf16[2048,512]{1,0:T(8,128)(2,1)} async-done(((bf16[128,512]{1,0:T(8,128)(2,1)}), bf16[2048,512]{1,0:T(8,128)(2,1)}) %all-gather.6.cloned.1.call-update) | async-done | bytes 2097168 | tf_op jit(solution)/shard_map/all_gather | solution.py:51
  135.9 2.0 fusion.53
  137.9 59.9 %all-gather.10.cloned.1.call-done = bf16[2048,512]{1,0:T(8,128)(2,1)} async-done(((bf16[128,512]{1,0:T(8,128)(2,1)}), bf16[2048,512]{1,0:T(8,128)(2,1)}) %all-gather.10.cloned.1.call-update) | async-done | bytes 2097168 | tf_op jit(solution)/shard_map/all_gather | solution.py:53
  197.9 2.0 fusion.50
  199.9 59.8 %all-gather.8.cloned.1.call-done = bf16[2048,512]{1,0:T(8,128)(2,1)} async-done(((bf16[128,512]{1,0:T(8,128)(2,1)}), bf16[2048,512]{1,0:T(8,128)(2,1)}) %all-gather.8.cloned.1.call-update) | async-done | bytes 2097168 | tf_op jit(solution)/shard_map/all_gather | solution.py:52
  259.7 2.0 fusion.21
  261.8 4.4 %multiply_add_fusion = f32[16,4,128,128]{3,2,1,0:T(8,128)S(1)} fusion(f32[16,4,128,128]{3,2,1,0:T(8,128)} %param.23, f32[16,4,128]{2,1,0:T(4,128)S(1)} %mul.124, f32[16,4,128]{2,1,0:T(4,128)S(1)} %broadcast_subtract_fusion, f32[16,4,128]{2,1,0:T(4,128)S(1)} %mul.120), kind=kLoop, calls=%fused_computation.6 | loop fusion | flops 3145728 | bytes 8486912 | tf_op jit(solution)/shard_map/add | solution.py:63
  266.2 2.0 copy-done
  268.2 3.7 %fusion.56 = f32[16,4,1,128]{3,2,1,0:T(1,128)S(1)} fusion(f32[16,4,128,1]{2,3,1,0:T(1,128)S(1)} %bitcast.58, f32[16,4,128,128]{3,2,1,0:T(8,128)S(1)} %multiply_add_fusion), kind=kOutput, calls=%fused_computation.66 | convolution fusion | flops 12582912 | bytes 4259840 | tf_op jit(solution)/shard_map/shk,shkv->shv/dot_general | solution.py:64
  272.1 1.3 convolution_convert_fusion.1
  273.4 16.6 %all-reduce.2.cloned.1.call-done = bf16[16,2048]{1,0:T(8,128)(2,1)} async-done(((bf16[16,2048]{1,0:T(8,128)(2,1)}), bf16[16,2048]{1,0:T(8,128)(2,1)}) %all-reduce.2.cloned.1.call-update) | async-done | bytes 65552 | tf_op jit(solution)/shard_map/psum | solution.py:72
  290.0 1.0 fusion.34
  291.5 22.1 %all_to_all.10 = bf16[16,6,2048]{2,1,0:T(8,128)(2,1)S(1)} all-to-all(bf16[16,6,2048]{2,1,0:T(8,128)(2,1)S(1)} %bitcast.55), channel_id=1, replica_groups=mesh['ep'=16,'tp'=2] {'ep'}, dimensions={0} | all-to-all | bytes 786432 | tf_op jit(solution)/shard_map/all_to_all | solution.py:98
  313.6 3.1 fusion.4
  316.7 5.9 %fusion.6 = bf16[16,6,2048]{2,0,1:T(8,128)(2,1)} fusion(bf16[1,1024,2048]{2,1,0:T(8,128)(2,1)} %param.29, bf16[1,2048,1024]{2,1,0:T(8,128)(2,1)} %param.28, f32[16,6,1024]{2,0,1:T(8,128)S(1)} %fusion.4, bf16[16,6,2048]{2,1,0:T(8,128)(2,1)S(1)} %all_to_all.10), kind=kOutput, calls=%fused_computation.7 | convolution fusion | flops 806092800 | bytes 9568256 | tf_op jit(solution)/shard_map/...f,fd->...d/dot_general | solution.py:104
  322.6 6.3 %reduce-scatter.2.cloned.1.call-done = bf16[16,6,1024]{2,0,1:T(8,128)(2,1)} async-done(((bf16[16,6,2048]{2,0,1:T(8,128)(2,1)}), bf16[16,6,1024]{2,0,1:T(8,128)(2,1)}) %reduce-scatter.2.cloned.1.call-update) | async-done | bytes 196624 | tf_op jit(solution)/shard_map/reduce_scatter | solution.py:107
  328.9 1.7 copy.60
  330.7 6.7 %all-to-all-start.1 = ((bf16[16,6,1024]{2,1,0:T(8,128)(2,1)}), bf16[16,6,1024]{2,1,0:T(8,128)(2,1)S(1)}, u32[]{:S(2)}, u32[]{:S(2)}) async-start(bf16[16,6,1024]{2,1,0:T(8,128)(2,1)} %copy.60), calls=%async_computation.2 | async-start | bytes 524288 | tf_op jit(solution)/shard_map/all_to_all | solution.py:110
  337.4 10.3 %all-to-all-done.1 = bf16[16,6,1024]{2,1,0:T(8,128)(2,1)S(1)} async-done(((bf16[16,6,1024]{2,1,0:T(8,128)(2,1)}), bf16[16,6,1024]{2,1,0:T(8,128)(2,1)S(1)}, u32[]{:S(2)}, u32[]{:S(2)}) %all-to-all-start.1) | async-done | bytes 196640 | tf_op jit(solution)/shard_map/all_to_all | solution.py:110
  347.8 0.9 fusion.16
  (49 shorter events, 5.6 us)
Async XLA Ops:
  7.2 128.7 %copy-start.1 = (bf16[16,2048]{1,0:T(8,128)(2,1)S(1)}, bf16[16,2048]{1,0:T(8,128)(2,1)}, u32[]{:S(2)}) copy-start(bf16[16,2048]{1,0:T(8,128)(2,1)} %param.15) | copy-start | bytes 196612
  7.2 128.7 %copy-start.2 = (f32[2048]{0:T(1024)S(1)}, f32[2048]{0:T(1024)}, u32[]{:S(2)}) copy-start(f32[2048]{0:T(1024)} %param.16) | copy-start | bytes 24580
  7.2 66.7 %all-gather.12.cloned.1.call-start = ((), (), s32[]{:S(2)}) async-start(), calls=%async_computation.8 | async-start | bytes 2228224 | tf_op jit(solution)/shard_map/all_gather | solution.py:69
  7.9 128.0 %all-gather.6.cloned.1.call-start = ((), (), s32[]{:S(2)}) async-start(), calls=%async_computation.3 | async-start | bytes 2228224 | tf_op jit(solution)/shard_map/all_gather | solution.py:51
  8.7 189.2 %all-gather.10.cloned.1.call-start = ((), (), s32[]{:S(2)}) async-start(), calls=%async_computation.5 | async-start | bytes 2228224 | tf_op jit(solution)/shard_map/all_gather | solution.py:53
  9.4 250.3 %all-gather.8.cloned.1.call-start = ((), (), s32[]{:S(2)}) async-start(), calls=%async_computation.4 | async-start | bytes 2228224 | tf_op jit(solution)/shard_map/all_gather | solution.py:52
  10.0 280.1 %all-reduce.2.cloned.1.call-start = ((), (), s32[]{:S(2)}) async-start(), calls=%async_computation.6 | async-start | bytes 131072 | tf_op jit(solution)/shard_map/psum | solution.py:72
  73.9 185.8 %copy-start.3 = (f32[512]{0:T(512)S(1)}, f32[512]{0:T(512)}, u32[]{:S(2)}) copy-start(f32[512]{0:T(512)} %param.20) | copy-start | bytes 6148
  266.2 2.0 copy-start
  266.2 5.8 %copy-start.5 = (f32[512]{0:T(512)S(1)}, f32[512]{0:T(512)}, u32[]{:S(2)}) copy-start(f32[512]{0:T(512)} %param.21) | copy-start | bytes 6148
  266.2 24.8 %copy-start.4 = (f32[2048]{0:T(1024)S(1)}, f32[2048]{0:T(1024)}, u32[]{:S(2)}) copy-start(f32[2048]{0:T(1024)} %param.24) | copy-start | bytes 24580
  273.4 55.6 %reduce-scatter.2.cloned.1.call-start = ((), (), s32[]{:S(2)}) async-start(), calls=%async_computation.7 | async-start | bytes 589824 | tf_op jit(solution)/shard_map/reduce_scatter | solution.py:107
  316.7 20.7 %copy-start.6 = (f32[16,2]{0,1:T(2,128)S(1)}, f32[16,2]{0,1:T(2,128)}, u32[]{:S(2)}) copy-start(f32[16,2]{0,1:T(2,128)} %param.26) | copy-start | bytes 388
  330.7 17.1 %all-to-all-start.1 = ((bf16[16,6,1024]{2,1,0:T(8,128)(2,1)}), bf16[16,6,1024]{2,1,0:T(8,128)(2,1)S(1)}, u32[]{:S(2)}, u32[]{:S(2)}) async-start(bf16[16,6,1024]{2,1,0:T(8,128)(2,1)} %copy.60), calls=%async_computation.2 | async-start | bytes 524288 | tf_op jit(solution)/shard_map/all_to_all | solution.py:110
Sparse Core Ops, SparseCore 0:
  10.8 63.0 all-gather.11
  76.7 59.1 all-gather.5
  138.7 59.1 all-gather.9
  200.5 59.1 all-gather.7
  273.5 16.4 all-reduce.1
  322.7 6.1 reduce-scatter.1
